TPU v7x, 32 devices: a whole 2x2x4 slice. The times are simulated.
32 devices in a mesh: fs: 32 (over z, y, x, core), tp: 1.
Axes of the slice: x: 2, y: 2, z: 4, core: 2. Of those that a mesh axis runs over, the one named last changes fastest.
Arguments:
- later_input: bfloat16 [6144, 2048], P(('fs', 'tp')), may hold values from -6 to 6
- earlier_input: bfloat16 [6144, 2048], P(('fs', 'tp')), may hold values from -6 to 6
- cotangent: bfloat16 [6144, 2048], P(('fs', 'tp')), may hold values from -6 to 6
- gate_weight: bfloat16 [2048, 3072], P('fs', 'tp'), may hold values from -0.125 to 0.125
- up_weight: bfloat16 [2048, 3072], P('fs', 'tp'), may hold values from -0.125 to 0.125
- down_weight: bfloat16 [2048, 3072], P('fs', 'tp'), may hold values from -0.109375 to 0.109375
- down_grad_sum: float32 [2048, 3072], P('fs', 'tp'), may hold values from -6 to 6
Outputs:
- later_output: bfloat16 [6144, 2048], P(('fs', 'tp'))
- earlier_grad_input: bfloat16 [6144, 2048], P(('fs', 'tp'))
- new_down_grad_sum: float32 [2048, 3072], P('fs', 'tp')
All inputs are finite; a program needn't handle non-finite values.
Results may differ from a plain program's by a relative error of at most 0.0057.
Values may be sent and summed in bfloat16 or wider, within the bound.
A program may use at most 192 MiB of HBM per device.

v0:
```python
import jax
import jax.numpy as jnp
from jax import lax
from jax.sharding import PartitionSpec as P

TOK_DEV = 192


def contract_last(leading, trailing):
    return lax.dot_general(
        leading, trailing, (((1,), (1,)), ((), ())), preferred_element_type=jnp.float32
    )


def add_parts(received, group):
    pieces = received.reshape(group, received.shape[0] // group, received.shape[1])
    return jnp.sum(pieces.astype(jnp.float32), axis=0).astype(jnp.bfloat16)


def shards(
    later_input, earlier_input, cotangent, gate_weight, up_weight, down_weight, down_grad_sum
):
    group = lax.axis_size("tp")
    later_rows, early_rows, grad_rows = (
        lax.all_gather(later_input, "tp", axis=0, tiled=True),
        lax.all_gather(earlier_input, "tp", axis=0, tiled=True),
        lax.all_gather(cotangent, "tp", axis=0, tiled=True),
    )
    columns = later_rows
    gate_later = jnp.dot(
        columns,
        lax.all_gather(gate_weight, "fs", axis=0, tiled=True),
        preferred_element_type=jnp.float32,
    )
    up_later = jnp.dot(
        columns,
        lax.all_gather(up_weight, "fs", axis=0, tiled=True),
        preferred_element_type=jnp.float32,
    )
    hidden_later = (jax.nn.silu(gate_later) * up_later).astype(jnp.bfloat16)
    partials = contract_last(hidden_later, lax.all_gather(down_weight, "fs", axis=0, tiled=True))
    gate_whole, up_whole, down_whole = (
        lax.all_gather(gate_weight, "fs", axis=0, tiled=True),
        lax.all_gather(up_weight, "fs", axis=0, tiled=True),
        lax.all_gather(down_weight, "fs", axis=0, tiled=True),
    )
    output_received = lax.all_to_all(
        partials.astype(jnp.bfloat16), "tp", split_axis=0, concat_axis=0, tiled=True
    )
    later_output = add_parts(output_received, group)
    gate_early = jnp.dot(early_rows, gate_whole, preferred_element_type=jnp.float32)
    up_early = jnp.dot(early_rows, up_whole, preferred_element_type=jnp.float32)
    sigmoid_gate = jax.nn.sigmoid(gate_early)
    activated = gate_early * sigmoid_gate
    hidden_early = (activated * up_early).astype(jnp.bfloat16)
    grad_hidden = jnp.dot(grad_rows, down_whole, preferred_element_type=jnp.float32)
    grad_gate = (
        grad_hidden * up_early * sigmoid_gate * (1.0 + gate_early * (1.0 - sigmoid_gate))
    ).astype(jnp.bfloat16)
    grad_up = (grad_hidden * activated).astype(jnp.bfloat16)
    input_partial = contract_last(grad_gate, gate_whole) + contract_last(grad_up, up_whole)
    input_received = lax.all_to_all(
        input_partial.astype(jnp.bfloat16), "tp", split_axis=0, concat_axis=0, tiled=True
    )
    earlier_grad_input = add_parts(input_received, group)
    columns = grad_rows
    summed = lax.psum_scatter(
        lax.dot_general(
            columns, hidden_early, (((0,), (0,)), ((), ())), preferred_element_type=jnp.float32
        ),
        "fs",
        scatter_dimension=0,
        tiled=True,
    )
    factor = (TOK_DEV * lax.axis_size("fs")) ** (-0.5)
    return (later_output, earlier_grad_input, down_grad_sum + summed * factor)


def solution(mesh):
    in_specs = (
        P(("fs", "tp"), None),
        P(("fs", "tp"), None),
        P(("fs", "tp"), None),
        P("fs", "tp"),
        P("fs", "tp"),
        P("fs", "tp"),
        P("fs", "tp"),
    )
    out_specs = (P(("fs", "tp"), None), P(("fs", "tp"), None), P("fs", "tp"))
    return jax.shard_map(shards, mesh=mesh, in_specs=in_specs, out_specs=out_specs, check_vma=False)
```

profile of v0, /device:TPU:0, one launch (start us, length us, event | category | flops | bytes accessed | tf_op | source)
XLA Modules:
  0.0 564.9 jit_solution(18282236890503028330)
XLA Ops:
  7.2 0.0 copy-start
  7.2 0.0 all-gather.4.cloned.1.call-start
  7.2 0.7 all-gather.4.cloned.1.call-update
  7.9 0.0 all-gather.6.cloned.1.call-start
  8.0 0.7 all-gather.6.cloned.1.call-update
  8.7 0.0 all-gather.8.cloned.1.call-start
  8.7 0.7 all-gather.8.cloned.1.call-update
  9.4 0.0 reduce-scatter.4.cloned.1.call-start
  9.4 99.3 %all-gather.4.cloned.1.call-done = bf16[2048,3072]{1,0:T(8,128)(2,1)} async-done(((bf16[64,3072]{1,0:T(8,128)(2,1)}), bf16[2048,3072]{1,0:T(8,128)(2,1)}) %all-gather.4.cloned.1.call-update) | async-done | bytes 12582928 | tf_op jit(solution)/shard_map/all_gather | solution.py:32
  108.8 6.2 %fusion.14 = f32[192,3072]{1,0:T(8,128)S(1)} fusion(bf16[192,2048]{1,0:T(8,128)(2,1)} %param.8, bf16[2048,3072]{1,0:T(8,128)(2,1)} %all-gather.4.cloned.1.call-done), kind=kOutput, calls=%fused_computation.21 | convolution fusion | flops 2415919104 | bytes 15728640 | tf_op jit(solution)/shard_map/dot_general | solution.py:51
  115.0 0.0 copy-start.2
  115.0 90.4 %all-gather.6.cloned.1.call-done = bf16[2048,3072]{1,0:T(8,128)(2,1)} async-done(((bf16[64,3072]{1,0:T(8,128)(2,1)}), bf16[2048,3072]{1,0:T(8,128)(2,1)}) %all-gather.6.cloned.1.call-update) | async-done | bytes 12582928 | tf_op jit(solution)/shard_map/all_gather | solution.py:37
  205.4 6.2 %fusion.13 = f32[192,3072]{1,0:T(8,128)S(1)} fusion(bf16[192,2048]{1,0:T(8,128)(2,1)} %param.8, bf16[2048,3072]{1,0:T(8,128)(2,1)} %all-gather.6.cloned.1.call-done), kind=kOutput, calls=%fused_computation.20 | convolution fusion | flops 2415919104 | bytes 15728640 | tf_op jit(solution)/shard_map/dot_general | solution.py:52
  211.7 1.4 copy-done.4
  213.1 0.0 copy-done
  213.1 10.2 %convolution_bitcast_fusion = f32[2048,3072]{0,1:T(8,128)} fusion(bf16[192,2048]{1,0:T(8,128)(2,1)S(1)} %copy-done, f32[192,3072]{1,0:T(8,128)S(1)} %fusion.13, f32[192,3072]{1,0:T(8,128)S(1)} %fusion.14), kind=kOutput, calls=%fused_computation | convolution fusion | flops 2419458048 | bytes 30670848 | tf_op jit(solution)/shard_map/dot_general | solution.py:68
  223.2 24.7 %copy.14 = f32[2048,3072]{1,0:T(8,128)} copy(f32[2048,3072]{0,1:T(8,128)} %convolution_bitcast_fusion) | data formatting | bytes 50331648
  248.0 0.0 reduce-scatter.4.cloned.1.call-update
  248.0 1.1 copy-done.6
  249.1 0.5 copy.12
  249.6 0.0 copy-start.7
  249.6 52.5 %all-gather.8.cloned.1.call-done = bf16[2048,3072]{1,0:T(8,128)(2,1)} async-done(((bf16[64,3072]{1,0:T(8,128)(2,1)}), bf16[2048,3072]{1,0:T(8,128)(2,1)}) %all-gather.8.cloned.1.call-update) | async-done | bytes 12582928 | tf_op jit(solution)/shard_map/all_gather | solution.py:41
  302.1 8.7 %fusion.12 = f32[192,3072]{1,0:T(8,128)} fusion(bf16[192,2048]{1,0:T(8,128)(2,1)S(1)} %copy-done, bf16[2048,3072]{1,0:T(8,128)(2,1)} %all-gather.8.cloned.1.call-done), kind=kOutput, calls=%fused_computation.19 | convolution fusion | flops 2415919104 | bytes 15728640 | tf_op jit(solution)/shard_map/dot_general | solution.py:56
  310.7 0.0 copy-done.7
  310.8 10.0 %fusion.11 = f32[192,3072]{1,0:T(8,128)} fusion(bf16[192,2048]{1,0:T(8,128)(2,1)S(1)} %copy-done.7, bf16[2048,3072]{1,0:T(8,128)(2,1)} %all-gather.4.cloned.1.call-done), kind=kOutput, calls=%fused_computation.18 | convolution fusion | flops 2415919104 | bytes 15728640 | tf_op jit(solution)/shard_map/dot_general | solution.py:30
  320.8 11.6 %fusion.3 = f32[192,2048]{1,0:T(8,128)S(1)} fusion(bf16[2048,3072]{1,0:T(8,128)(2,1)} %all-gather.4.cloned.1.call-done, f32[192,3072]{1,0:T(8,128)S(1)} %copy-done.3, f32[192,3072]{1,0:T(8,128)} %fusion.12, f32[192,3072]{1,0:T(8,128)S(1)} %copy-done.5), kind=kOutput, calls=%fused_computation.12 | convolution fusion | flops 2421817344 | bytes 21233664 | tf_op jit(solution)/shard_map/dot_general | solution.py:10
  332.3 12.1 %fusion.1 = bf16[192,2048]{1,0:T(8,128)(2,1)} fusion(f32[192,2048]{1,0:T(8,128)S(1)} %fusion.3, bf16[2048,3072]{1,0:T(8,128)(2,1)} %all-gather.6.cloned.1.call-done, f32[192,3072]{1,0:T(8,128)} %fusion.12, f32[192,3072]{1,0:T(8,128)S(1)} %copy-done.3), kind=kOutput, calls=%fused_computation.4 | convolution fusion | flops 2420244480 | bytes 19660800 | tf_op jit(solution)/shard_map/dot_general | solution.py:10
  344.4 19.8 %convolution_convert_fusion = bf16[192,2048]{1,0:T(8,128)(2,1)} fusion(bf16[2048,3072]{1,0:T(8,128)(2,1)} %all-gather.8.cloned.1.call-done, bf16[192,2048]{1,0:T(8,128)(2,1)S(1)} %copy-done.7, bf16[2048,3072]{1,0:T(8,128)(2,1)} %all-gather.6.cloned.1.call-done, f32[192,3072]{1,0:T(8,128)} %fusion.11), kind=kOutput, calls=%fused_computation.5 | convolution fusion | flops 4835770368 | bytes 29097984 | tf_op jit(solution)/shard_map/dot_general | solution.py:10
  364.2 185.8 %reduce-scatter.4.cloned.1.call-done = f32[64,3072]{1,0:T(8,128)} async-done(((f32[2048,3072]{1,0:T(8,128)}), f32[64,3072]{1,0:T(8,128)}) %reduce-scatter.4.cloned.1.call-update) | async-done | bytes 786448
  550.0 2.8 copy.15
  552.8 2.8 multiply_add_fusion
  555.7 2.7 copy.13
  (9 shorter events, 0.0 us)
Async XLA Ops:
  7.2 205.9 %copy-start = (bf16[192,2048]{1,0:T(8,128)(2,1)S(1)}, bf16[192,2048]{1,0:T(8,128)(2,1)}, u32[]{:S(2)}) copy-start(bf16[192,2048]{1,0:T(8,128)(2,1)} %param.9) | copy-start | bytes 2359300
  7.2 101.6 %all-gather.4.cloned.1.call-start = ((), (), s32[]{:S(2)}) async-start(), calls=%async_computation.1 | async-start | bytes 12976128 | tf_op jit(solution)/shard_map/all_gather | solution.py:32
  7.9 197.5 %all-gather.6.cloned.1.call-start = ((), (), s32[]{:S(2)}) async-start(), calls=%async_computation.2 | async-start | bytes 12976128 | tf_op jit(solution)/shard_map/all_gather | solution.py:37
  8.7 293.4 %all-gather.8.cloned.1.call-start = ((), (), s32[]{:S(2)}) async-start(), calls=%async_computation.3 | async-start | bytes 12976128 | tf_op jit(solution)/shard_map/all_gather | solution.py:41
  9.4 540.6 %reduce-scatter.4.cloned.1.call-start = ((), (), s32[]{:S(2)}) async-start(), calls=%async_computation.4 | async-start | bytes 25952256
  115.0 96.7 %copy-start.2 = (f32[192,3072]{1,0:T(8,128)}, f32[192,3072]{1,0:T(8,128)S(1)}, u32[]{:S(2)}) copy-start(f32[192,3072]{1,0:T(8,128)S(1)} %fusion.14) | copy-start | bytes 7077892
  211.7 1.4 copy-start.4
  248.0 1.1 copy-start.6
  249.6 61.2 %copy-start.7 = (bf16[192,2048]{1,0:T(8,128)(2,1)S(1)}, bf16[192,2048]{1,0:T(8,128)(2,1)}, u32[]{:S(2)}) copy-start(bf16[192,2048]{1,0:T(8,128)(2,1)} %param.7) | copy-start | bytes 2359300
  310.7 10.0 %copy-start.3 = (f32[192,3072]{1,0:T(8,128)S(1)}, f32[192,3072]{1,0:T(8,128)}, u32[]{:S(2)}) copy-start(f32[192,3072]{1,0:T(8,128)} %copy-done.2) | copy-start | bytes 7077892
  310.7 10.0 %copy-start.5 = (f32[192,3072]{1,0:T(8,128)S(1)}, f32[192,3072]{1,0:T(8,128)}, u32[]{:S(2)}) copy-start(f32[192,3072]{1,0:T(8,128)} %copy-done.4) | copy-start | bytes 7077892
  552.8 5.6 copy-start.1
Sparse Core Ops, SparseCore 0:
  10.9 97.8 all-gather.3
  111.6 93.7 all-gather.5
  208.3 93.7 all-gather.7
  308.4 241.6 reduce-scatter.3
where the time goes:
time: 566 us; the launch traced here: 565 us
  waiting for transfers between devices  430 us (76%)
  matrix products  84.8 us (15%)
  local copies, waits for them, and re-layouts  33.3 us (6%)
  between operations  13.8 us (2%)
    unnamed x5, waiting for transfers between devices  188 us
    all_gather x1, waiting for transfers between devices, shards(): lax.all_gather(gate_weight, 'fs', axis=0, tiled=True)  99.3 us
    all_gather x1, waiting for transfers between devices, shards(): lax.all_gather(up_weight, 'fs', axis=0, tiled=True)  90.4 us
    all_gather x1, waiting for transfers between devices, shards(): lax.all_gather(down_weight, 'fs', axis=0, tiled=True)  52.5 us
    dot_general x3, matrix products, contract_last(): lax.dot_general(leading, trailing, (((1,), (1,)), ((), ())), preferred_el...  43.4 us
    unnamed x20, local copies, waits for them, and re-layouts  33.3 us
  transfers between devices with their start and end apart: 4, of which 4 were waited for; matrix products, arithmetic and copies ran while one was open for 19% of the time, Pallas kernels for 0%

commit v1 on v0

--- a/solution.py
+++ b/solution.py
@@ -3,7 +3,7 @@
 from jax import lax
 from jax.sharding import PartitionSpec as P
 
-TOK_DEV = 192
+QUAD = 4
 
 
 def contract_last(leading, trailing):
@@ -72,8 +72,91 @@
         scatter_dimension=0,
         tiled=True,
     )
-    factor = (TOK_DEV * lax.axis_size("fs")) ** (-0.5)
+    factor = (later_rows.shape[0] * lax.axis_size("fs")) ** (-0.5)
     return (later_output, earlier_grad_input, down_grad_sum + summed * factor)
+
+def quads_of(total):
+    return [[first + place for place in range(QUAD)] for first in range(0, total, QUAD)]
+
+
+def lanes_of(total):
+    return [[first + place for first in range(0, total, QUAD)] for place in range(QUAD)]
+
+
+def swap(value, bit):
+    total = lax.axis_size("fs")
+    return lax.ppermute(value, "fs", [(index, index ^ bit) for index in range(total)])
+
+
+def gather_tokens(rows):
+    far = swap(rows, 2)
+    return jnp.concatenate([rows, swap(rows, 1), far, swap(far, 1)], axis=0)
+
+
+def return_tokens(partial):
+    blocks = partial.astype(jnp.bfloat16).reshape(QUAD, -1, partial.shape[1])
+    mine = partial.reshape(blocks.shape)
+    near = swap(jnp.stack([blocks[1], blocks[3]]), 1).astype(jnp.float32)
+    far = swap((mine[2] + near[1]).astype(jnp.bfloat16), 2)
+    return (mine[0] + near[0] + far.astype(jnp.float32)).astype(jnp.bfloat16)
+
+
+def gather_weight(weight):
+    total = lax.axis_size("fs")
+    part = lax.all_to_all(
+        weight, "fs", split_axis=1, concat_axis=0, tiled=True, axis_index_groups=quads_of(total)
+    )
+    return lax.all_gather(part, "fs", axis=0, tiled=True, axis_index_groups=lanes_of(total))
+
+
+def quad_shards(
+    later_input, earlier_input, cotangent, gate_weight, up_weight, down_weight, down_grad_sum
+):
+    total = lax.axis_size("fs")
+    gate_whole = gather_weight(gate_weight)
+    up_whole = gather_weight(up_weight)
+    down_whole = gather_weight(down_weight)
+    early_rows = gather_tokens(earlier_input)
+    grad_rows = gather_tokens(cotangent)
+    later_rows = gather_tokens(later_input)
+
+    gate_early = jnp.dot(early_rows, gate_whole, preferred_element_type=jnp.float32)
+    up_early = jnp.dot(early_rows, up_whole, preferred_element_type=jnp.float32)
+    sigmoid_gate = jax.nn.sigmoid(gate_early)
+    activated = gate_early * sigmoid_gate
+    hidden_early = (activated * up_early).astype(jnp.bfloat16)
+    partial_sum = lax.dot_general(
+        grad_rows, hidden_early, (((0,), (0,)), ((), ())), preferred_element_type=jnp.float32
+    ).astype(jnp.bfloat16)
+    summed = lax.psum_scatter(
+        partial_sum,
+        "fs",
+        scatter_dimension=0,
+        tiled=True,
+        axis_index_groups=lanes_of(total),
+    )
+    gate_later = jnp.dot(later_rows, gate_whole, preferred_element_type=jnp.float32)
+    up_later = jnp.dot(later_rows, up_whole, preferred_element_type=jnp.float32)
+    hidden_later = (jax.nn.silu(gate_later) * up_later).astype(jnp.bfloat16)
+
+    grad_hidden = jnp.dot(grad_rows, down_whole, preferred_element_type=jnp.float32)
+    grad_gate = (
+        grad_hidden * up_early * sigmoid_gate * (1.0 + gate_early * (1.0 - sigmoid_gate))
+    ).astype(jnp.bfloat16)
+    grad_up = (grad_hidden * activated).astype(jnp.bfloat16)
+    later_output = return_tokens(contract_last(hidden_later, down_whole))
+    earlier_grad_input = return_tokens(
+        contract_last(grad_gate, gate_whole) + contract_last(grad_up, up_whole)
+    )
+    own_rows = lax.all_to_all(
+        summed, "fs", split_axis=0, concat_axis=1, tiled=True, axis_index_groups=quads_of(total)
+    )
+    factor = (later_input.shape[0] * total) ** (-0.5)
+    return (
+        later_output,
+        earlier_grad_input,
+        down_grad_sum + own_rows.astype(jnp.float32) * factor,
+    )
 
 
 def solution(mesh):
@@ -87,4 +170,6 @@
         P("fs", "tp"),
     )
     out_specs = (P(("fs", "tp"), None), P(("fs", "tp"), None), P("fs", "tp"))
-    return jax.shard_map(shards, mesh=mesh, in_specs=in_specs, out_specs=out_specs, check_vma=False)
+    split = mesh.shape["tp"] == 1 and mesh.shape["fs"] % (2 * QUAD) == 0
+    body = quad_shards if split else shards
+    return jax.shard_map(body, mesh=mesh, in_specs=in_specs, out_specs=out_specs, check_vma=False)

time: 566 us -> 324 us (0.57)
  waiting for transfers between devices: 430 us -> 198 us
  matrix products: 84.8 us -> 43.1 us
  blocking collectives: 0 us -> 32.5 us
  local copies, waits for them, and re-layouts: 33.3 us -> 12.8 us
  other arithmetic: 2.83 us -> 13.9 us
  starting transfers between devices: 0.15 us -> 8.86 us
    unnamed x5 -> x4, waiting for transfers between devices: 188 us -> 0.07 us
    all_gather x3, waiting for transfers between devices: 242 us -> 94.2 us  [gather_weight(): lax.all_gather(part, 'fs', axis=0, tiled=True, axis_index_groups=lanes_of...]
    ppermute x0 -> x13, waiting for transfers between devices: none -> 66.4 us  [swap(): lax.ppermute(value, 'fs', [(index, index ^ bit) for index in range(total)])]
    reduce_scatter x0 -> x1, waiting for transfers between devices: none -> 33.3 us  [quad_shards(): lax.psum_scatter(partial_sum, 'fs', scatter_dimension=0, tiled=True, axis...]
    all_to_all x0 -> x3, blocking collectives: none -> 32.5 us  [gather_weight(): lax.all_to_all(weight, 'fs', split_axis=1, concat_axis=0, tiled=True, axi...]
    dot_general x3, matrix products: 43.4 us -> 18.9 us  [contract_last(): lax.dot_general(leading, trailing, (((1,), (1,)), ((), ())), preferred_el...]
    unnamed x20 -> x41, local copies, waits for them, and re-layouts: 33.3 us -> 9.03 us
    dot_general x5, matrix products: 41.3 us -> 24.3 us  [the longest x1 6.9 us: quad_shards(): jnp.dot(later_rows, gate_whole, preferred_element_type=jnp.float32)]
  transfers between devices with their start and end apart: 4 -> 18, of which waited for: 4 -> 9; matrix products, arithmetic and copies ran while one was open for 19% -> 15% of each run, Pallas kernels for 0% -> 0%
where the time goes in v1:
time: 324 us
  waiting for transfers between devices  198 us (61%)
  matrix products  43.1 us (13%)
  blocking collectives  32.5 us (10%)
  between operations  14.2 us (4%)
  other arithmetic  13.9 us (4%)
  local copies, waits for them, and re-layouts  12.8 us (4%)
  starting transfers between devices  8.86 us (3%)
    all_gather x3, waiting for transfers between devices, gather_weight(): lax.all_gather(part, 'fs', axis=0, tiled=True, axis_index_groups=lanes_of...  94.2 us
    ppermute x13, waiting for transfers between devices, swap(): lax.ppermute(value, 'fs', [(index, index ^ bit) for index in range(total)])  66.4 us
    reduce_scatter x1, waiting for transfers between devices, quad_shards(): lax.psum_scatter(partial_sum, 'fs', scatter_dimension=0, tiled=True, axis...  33.3 us
    all_to_all x3, blocking collectives, gather_weight(): lax.all_to_all(weight, 'fs', split_axis=1, concat_axis=0, tiled=True, axi...  32.5 us
    dot_general x3, matrix products, contract_last(): lax.dot_general(leading, trailing, (((1,), (1,)), ((), ())), preferred_el...  18.9 us
    unnamed x41, local copies, waits for them, and re-layouts  9.03 us
    dot_general x1, matrix products, quad_shards(): jnp.dot(later_rows, gate_whole, preferred_element_type=jnp.float32)  6.9 us
    dot_general x1, matrix products, quad_shards(): lax.dot_general(grad_rows, hidden_early, (((0,), (0,)), ((), ())), prefer...  6.58 us
  transfers between devices with their start and end apart: 18, of which 9 were waited for; matrix products, arithmetic and copies ran while one was open for 15% of the time, Pallas kernels for 0%

profile of v1, /device:TPU:0, one launch (start us, length us, event | category | flops | bytes accessed | tf_op | source)
XLA Modules:
  0.0 323.9 jit_solution(15146005721328778845)
XLA Ops:
  7.3 1.2 copy.29
  8.4 11.6 %all_to_all.70 = bf16[64,4,768]{2,0,1:T(8,128)(2,1)} all-to-all(bf16[64,4,768]{2,0,1:T(8,128)(2,1)S(1)} %bitcast.80), channel_id=1, replica_groups={{0,1,2,3},{4,5,6,7},{8,9,10,11},{12,13,14,15},{16,17,18,19},{20,21,22,2..., dimensions={1} | all-to-all | bytes 786432 | tf_op jit(solution)/shard_map/all_to_all | solution.py:106
  20.1 1.0 copy.27
  21.1 10.5 %all_to_all.71 = bf16[64,4,768]{2,0,1:T(8,128)(2,1)} all-to-all(bf16[64,4,768]{2,0,1:T(8,128)(2,1)S(1)} %bitcast.81), channel_id=1, replica_groups={{0,1,2,3},{4,5,6,7},{8,9,10,11},{12,13,14,15},{16,17,18,19},{20,21,22,2..., dimensions={1} | all-to-all | bytes 786432 | tf_op jit(solution)/shard_map/all_to_all | solution.py:106
  31.7 10.5 %all_to_all.72 = bf16[64,4,768]{2,0,1:T(8,128)(2,1)} all-to-all(bf16[64,4,768]{2,0,1:T(8,128)(2,1)S(1)} %bitcast.82), channel_id=1, replica_groups={{0,1,2,3},{4,5,6,7},{8,9,10,11},{12,13,14,15},{16,17,18,19},{20,21,22,2..., dimensions={1} | all-to-all | bytes 786432 | tf_op jit(solution)/shard_map/all_to_all | solution.py:106
  42.8 1.6 collective-permute-start.9
  46.4 16.4 %collective-permute-done.1 = bf16[192,2048]{1,0:T(8,128)(2,1)S(1)} collective-permute-done((bf16[192,2048]{1,0:T(8,128)(2,1)S(1)}, bf16[192,2048]{1,0:T(8,128)(2,1)S(1)}, u32[]{:S(2)}, u32[]{:S(2)}) %collective-permute-start.1) | collective-permute-done | bytes 786464 | tf_op jit(solution)/shard_map/ppermute | solution.py:88
  62.8 16.8 %collective-permute-done.9 = bf16[192,2048]{1,0:T(8,128)(2,1)S(1)} collective-permute-done((bf16[192,2048]{1,0:T(8,128)(2,1)S(1)}, bf16[192,2048]{1,0:T(8,128)(2,1)S(1)}, u32[]{:S(2)}, u32[]{:S(2)}) %collective-permute-start.9) | collective-permute-done | bytes 786464 | tf_op jit(solution)/shard_map/ppermute | solution.py:88
  80.0 16.0 %collective-permute-done.6 = bf16[192,2048]{1,0:T(8,128)(2,1)S(1)} collective-permute-done((bf16[192,2048]{1,0:T(8,128)(2,1)S(1)}, bf16[192,2048]{1,0:T(8,128)(2,1)S(1)}, u32[]{:S(2)}, u32[]{:S(2)}) %collective-permute-start.6) | collective-permute-done | bytes 786464 | tf_op jit(solution)/shard_map/ppermute | solution.py:88
  98.3 1.4 copy-done.11
  101.6 6.9 %fusion.25 = f32[768,768]{1,0:T(8,128)} fusion(bf16[768,2048]{1,0:T(8,128)(2,1)} %copy-done.11, bf16[2048,768]{1,0:T(8,128)(2,1)} %all-gather.4.cloned.1.call-done), kind=kOutput, calls=%fused_computation.55 | convolution fusion | flops 2415919104 | bytes 8650752 | tf_op jit(solution)/shard_map/dot_general | solution.py:138
  108.5 33.3 %all-gather.8.cloned.1.call-done = bf16[2048,768]{1,0:T(8,128)(2,1)} async-done(((bf16[256,768]{1,0:T(8,128)(2,1)}), bf16[2048,768]{1,0:T(8,128)(2,1)}) %all-gather.8.cloned.1.call-update) | async-done | bytes 3145744 | tf_op jit(solution)/shard_map/all_gather | solution.py:109
  141.8 60.9 %all-gather.6.cloned.1.call-done = bf16[2048,768]{1,0:T(8,128)(2,1)} async-done(((bf16[256,768]{1,0:T(8,128)(2,1)}), bf16[2048,768]{1,0:T(8,128)(2,1)}) %all-gather.6.cloned.1.call-update) | async-done | bytes 3145744 | tf_op jit(solution)/shard_map/all_gather | solution.py:109
  202.7 12.9 %fusion.21 = (bf16[768,2048]{1,0:T(8,128)(2,1)S(1)}, f32[768,2048]{1,0:T(8,128)}) fusion(bf16[2048,768]{1,0:T(8,128)(2,1)} %all-gather.8.cloned.1.call-done, f32[768,768]{1,0:T(8,128)} %fusion.25, bf16[768,2048]{1,0:T(8,128)(2,1)} %copy-done.11, bf16[2048,768]{1,0:T(8,128)(2,1)} %all-gather.6.cloned.1.call-done), kind=kOutput, calls=%fused_computation.52 | convolution fusion | flops 4836950016 | bytes 21233664 | tf_op jit(solution)/shard_map/dot_general | solution.py:10
  215.8 1.3 pad_maximum_fusion
  219.0 2.6 fusion.28
  221.6 2.6 fusion.27
  224.3 1.4 copy-done.14
  225.7 6.6 %convolution_convert_fusion = bf16[2048,768]{1,0:T(8,128)(2,1)} fusion(bf16[768,2048]{1,0:T(8,128)(2,1)} %constant_dynamic-update-slice_fusion.4, f32[768,768]{1,0:T(8,128)S(1)} %fusion.27, f32[768,768]{1,0:T(8,128)S(1)} %fusion.28), kind=kOutput, calls=%fused_computation.1 | convolution fusion | flops 2421030912 | bytes 11010048 | tf_op jit(solution)/shard_map/dot_general | solution.py:128
  232.3 5.6 %fusion.26 = f32[768,768]{1,0:T(8,128)S(1)} fusion(bf16[768,2048]{1,0:T(8,128)(2,1)} %constant_dynamic-update-slice_fusion.4, bf16[2048,768]{1,0:T(8,128)(2,1)} %all-gather.8.cloned.1.call-done), kind=kOutput, calls=%fused_computation.56 | convolution fusion | flops 2415919104 | bytes 8650752 | tf_op jit(solution)/shard_map/dot_general | solution.py:142
  237.9 3.3 %fusion.12 = f32[768,2048]{1,0:T(8,128)S(1)} fusion(bf16[2048,768]{1,0:T(8,128)(2,1)S(1)} %copy-done.13, f32[768,768]{1,0:T(8,128)S(1)} %copy-done.3, f32[768,768]{1,0:T(8,128)S(1)} %fusion.26, f32[768,768]{1,0:T(8,128)S(1)} %copy-done.15), kind=kOutput, calls=%fused_computation.25 | convolution fusion | flops 2421817344 | bytes 16515072 | tf_op jit(solution)/shard_map/dot_general | solution.py:10
  241.3 2.7 fusion.22
  244.4 3.0 convert_element_type.52
  247.4 1.6 fusion.7
  249.0 1.5 collective-permute-start.4
  250.9 1.1 fusion.2
  252.5 16.9 %collective-permute-done.4 = bf16[192,2048]{1,0:T(8,128)(2,1)S(1)} collective-permute-done((bf16[192,2048]{1,0:T(8,128)(2,1)S(1)}, bf16[192,2048]{1,0:T(8,128)(2,1)S(1)}, u32[]{:S(2)}, u32[]{:S(2)}) %collective-permute-start.4) | collective-permute-done | bytes 786464 | tf_op jit(solution)/shard_map/ppermute | solution.py:88
  269.5 2.6 fusion.10
  272.1 33.3 %reduce-scatter.2.cloned.1.call-done = bf16[256,768]{1,0:T(8,128)(2,1)} async-done(((bf16[2048,768]{1,0:T(8,128)(2,1)}), bf16[256,768]{1,0:T(8,128)(2,1)}) %reduce-scatter.2.cloned.1.call-update) | async-done | bytes 393232 | tf_op jit(solution)/shard_map/reduce_scatter | solution.py:131
  305.4 3.5 %all-to-all-start.3 = ((bf16[4,64,768]{2,1,0:T(8,128)(2,1)}), bf16[4,64,768]{2,1,0:T(8,128)(2,1)S(1)}, u32[]{:S(2)}, u32[]{:S(2)}) async-start(bf16[4,64,768]{2,1,0:T(8,128)(2,1)} %bitcast.86), calls=%async_computation.4 | async-start | bytes 786432 | tf_op jit(solution)/shard_map/all_to_all | solution.py:151
  308.9 2.8 fusion.5
  311.7 4.6 %all-to-all-done.3 = bf16[4,64,768]{2,1,0:T(8,128)(2,1)S(1)} async-done(((bf16[4,64,768]{2,1,0:T(8,128)(2,1)}), bf16[4,64,768]{2,1,0:T(8,128)(2,1)S(1)}, u32[]{:S(2)}, u32[]{:S(2)}) %all-to-all-start.3) | async-done | bytes 393248 | tf_op jit(solution)/shard_map/all_to_all | solution.py:151
  (79 shorter events, 11.8 us)
Async XLA Ops:
  7.2 24.5 %copy-start.8 = (bf16[64,3072]{1,0:T(8,128)(2,1)S(1)}, bf16[64,3072]{1,0:T(8,128)(2,1)}, u32[]{:S(2)}) copy-start(bf16[64,3072]{1,0:T(8,128)(2,1)} %param.11) | copy-start | bytes 1179652
  7.2 35.1 %copy-start.4 = (bf16[192,2048]{1,0:T(8,128)(2,1)S(1)}, bf16[192,2048]{1,0:T(8,128)(2,1)}, u32[]{:S(2)}) copy-start(bf16[192,2048]{1,0:T(8,128)(2,1)} %param.7) | copy-start | bytes 2359300
  7.2 35.6 %copy-start.5 = (bf16[192,2048]{1,0:T(8,128)(2,1)S(1)}, bf16[192,2048]{1,0:T(8,128)(2,1)}, u32[]{:S(2)}) copy-start(bf16[192,2048]{1,0:T(8,128)(2,1)} %param.8) | copy-start | bytes 2359300
  7.2 37.2 %copy-start.6 = (bf16[192,2048]{1,0:T(8,128)(2,1)S(1)}, bf16[192,2048]{1,0:T(8,128)(2,1)}, u32[]{:S(2)}) copy-start(bf16[192,2048]{1,0:T(8,128)(2,1)} %param.9) | copy-start | bytes 2359300
  7.2 94.4 %all-gather.4.cloned.1.call-start = ((), (), s32[]{:S(2)}) async-start(), calls=%async_computation.5 | async-start | bytes 3538944 | tf_op jit(solution)/shard_map/all_gather | solution.py:109
  20.0 121.8 %all-gather.8.cloned.1.call-start = ((), (), s32[]{:S(2)}) async-start(), calls=%async_computation.7 | async-start | bytes 3538944 | tf_op jit(solution)/shard_map/all_gather | solution.py:109
  31.6 171.1 %all-gather.6.cloned.1.call-start = ((), (), s32[]{:S(2)}) async-start(), calls=%async_computation.6 | async-start | bytes 3538944 | tf_op jit(solution)/shard_map/all_gather | solution.py:109
  42.2 263.2 %reduce-scatter.2.cloned.1.call-start = ((), (), s32[]{:S(2)}) async-start(), calls=%async_computation.8 | async-start | bytes 3538944 | tf_op jit(solution)/shard_map/reduce_scatter | solution.py:131
  42.2 3.8 %collective-permute-start = (bf16[192,2048]{1,0:T(8,128)(2,1)S(1)}, bf16[192,2048]{1,0:T(8,128)(2,1)S(1)}, u32[]{:S(2)}, u32[]{:S(2)}) collective-permute-start(bf16[192,2048]{1,0:T(8,128)(2,1)S(1)} %copy-done.4), channel_id=1, source_target_pairs={{0,1},{1,0},{2,3},{3,2},{4,5},{5,4},{6,7},{7,6},{8,9},{9,8},{10,11... | collective-permute-start | bytes 2359304 | tf_op jit(solution)/shard_map/ppermute | solution.py:88
  42.3 20.5 %collective-permute-start.1 = (bf16[192,2048]{1,0:T(8,128)(2,1)S(1)}, bf16[192,2048]{1,0:T(8,128)(2,1)S(1)}, u32[]{:S(2)}, u32[]{:S(2)}) collective-permute-start(bf16[192,2048]{1,0:T(8,128)(2,1)S(1)} %copy-done.4), channel_id=1, source_target_pairs={{0,2},{1,3},{2,0},{3,1},{4,6},{5,7},{6,4},{7,5},{8,10},{9,11},{10,... | collective-permute-start | bytes 2359304 | tf_op jit(solution)/shard_map/ppermute | solution.py:88
  42.8 36.9 %collective-permute-start.9 = (bf16[192,2048]{1,0:T(8,128)(2,1)S(1)}, bf16[192,2048]{1,0:T(8,128)(2,1)S(1)}, u32[]{:S(2)}, u32[]{:S(2)}) collective-permute-start(bf16[192,2048]{1,0:T(8,128)(2,1)S(1)} %copy-done.5), channel_id=1, source_target_pairs={{0,2},{1,3},{2,0},{3,1},{4,6},{5,7},{6,4},{7,5},{8,10},{9,11},{10,... | collective-permute-start | bytes 2359304 | tf_op jit(solution)/shard_map/ppermute | solution.py:88
  44.4 35.4 %collective-permute-start.8 = (bf16[192,2048]{1,0:T(8,128)(2,1)S(1)}, bf16[192,2048]{1,0:T(8,128)(2,1)S(1)}, u32[]{:S(2)}, u32[]{:S(2)}) collective-permute-start(bf16[192,2048]{1,0:T(8,128)(2,1)S(1)} %copy-done.5), channel_id=1, source_target_pairs={{0,1},{1,0},{2,3},{3,2},{4,5},{5,4},{6,7},{7,6},{8,9},{9,8},{10,11... | collective-permute-start | bytes 2359304 | tf_op jit(solution)/shard_map/ppermute | solution.py:88
  44.4 51.6 %collective-permute-start.5 = (bf16[192,2048]{1,0:T(8,128)(2,1)S(1)}, bf16[192,2048]{1,0:T(8,128)(2,1)S(1)}, u32[]{:S(2)}, u32[]{:S(2)}) collective-permute-start(bf16[192,2048]{1,0:T(8,128)(2,1)S(1)} %copy-done.6), channel_id=1, source_target_pairs={{0,1},{1,0},{2,3},{3,2},{4,5},{5,4},{6,7},{7,6},{8,9},{9,8},{10,11... | collective-permute-start | bytes 2359304 | tf_op jit(solution)/shard_map/ppermute | solution.py:88
  46.0 50.0 %collective-permute-start.6 = (bf16[192,2048]{1,0:T(8,128)(2,1)S(1)}, bf16[192,2048]{1,0:T(8,128)(2,1)S(1)}, u32[]{:S(2)}, u32[]{:S(2)}) collective-permute-start(bf16[192,2048]{1,0:T(8,128)(2,1)S(1)} %copy-done.6), channel_id=1, source_target_pairs={{0,2},{1,3},{2,0},{3,1},{4,6},{5,7},{6,4},{7,5},{8,10},{9,11},{10,... | collective-permute-start | bytes 2359304 | tf_op jit(solution)/shard_map/ppermute | solution.py:88
  62.8 35.1 %collective-permute-start.2 = (bf16[192,2048]{1,0:T(8,128)(2,1)S(1)}, bf16[192,2048]{1,0:T(8,128)(2,1)S(1)}, u32[]{:S(2)}, u32[]{:S(2)}) collective-permute-start(bf16[192,2048]{1,0:T(8,128)(2,1)S(1)} %collective-permute-done.1), channel_id=1, source_target_pairs={{0,1},{1,0},{2,3},{3,2},{4,5},{5,4},{6,7},{7,6},{8,9},{9,8},{10,11... | collective-permute-start | bytes 2359304 | tf_op jit(solution)/shard_map/ppermute | solution.py:88
  79.7 18.4 %collective-permute-start.10 = (bf16[192,2048]{1,0:T(8,128)(2,1)S(1)}, bf16[192,2048]{1,0:T(8,128)(2,1)S(1)}, u32[]{:S(2)}, u32[]{:S(2)}) collective-permute-start(bf16[192,2048]{1,0:T(8,128)(2,1)S(1)} %collective-permute-done.9), channel_id=1, source_target_pairs={{0,1},{1,0},{2,3},{3,2},{4,5},{5,4},{6,7},{7,6},{8,9},{9,8},{10,11... | collective-permute-start | bytes 2359304 | tf_op jit(solution)/shard_map/ppermute | solution.py:88
  96.0 2.3 collective-permute-start.7
  98.1 2.5 copy-start.9
  215.6 2.5 copy-start.10
  215.6 3.4 %copy-start.12 = (bf16[2048,768]{1,0:T(8,128)(2,1)S(1)}, bf16[2048,768]{1,0:T(8,128)(2,1)}, u32[]{:S(2)}) copy-start(bf16[2048,768]{1,0:T(8,128)(2,1)} %all-gather.4.cloned.1.call-done) | copy-start | bytes 9437188
  217.1 4.5 %copy-start.1 = (bf16[2048,768]{1,0:T(8,128)(2,1)S(1)}, bf16[2048,768]{1,0:T(8,128)(2,1)}, u32[]{:S(2)}) copy-start(bf16[2048,768]{1,0:T(8,128)(2,1)} %all-gather.6.cloned.1.call-done) | copy-start | bytes 9437188
  217.1 27.3 %collective-permute-start.3 = (bf16[2,192,2048]{2,1,0:T(8,128)(2,1)}, bf16[2,192,2048]{2,1,0:T(8,128)(2,1)}, u32[]{:S(2)}, u32[]{:S(2)}) collective-permute-start(bf16[2,192,2048]{2,1,0:T(8,128)(2,1)} %pad_maximum_fusion), channel_id=1, source_target_pairs={{0,1},{1,0},{2,3},{3,2},{4,5},{5,4},{6,7},{7,6},{8,9},{9,8},{10,11... | collective-permute-start | bytes 4718600 | tf_op jit(solution)/shard_map/ppermute | solution.py:88
  221.6 2.6 copy-start.2
  232.3 5.6 %copy-start.3 = (f32[768,768]{1,0:T(8,128)S(1)}, f32[768,768]{1,0:T(8,128)}, u32[]{:S(2)}) copy-start(f32[768,768]{1,0:T(8,128)} %copy-done.2) | copy-start | bytes 7077892
  232.3 5.6 %copy-start.13 = (bf16[2048,768]{1,0:T(8,128)(2,1)S(1)}, bf16[2048,768]{1,0:T(8,128)(2,1)}, u32[]{:S(2)}) copy-start(bf16[2048,768]{1,0:T(8,128)(2,1)} %all-gather.4.cloned.1.call-done) | copy-start | bytes 9437188
  232.3 5.6 %copy-start.15 = (f32[768,768]{1,0:T(8,128)S(1)}, f32[768,768]{1,0:T(8,128)}, u32[]{:S(2)}) copy-start(f32[768,768]{1,0:T(8,128)} %copy-done.14) | copy-start | bytes 7077892
  243.9 7.0 %copy-start = (f32[768,2048]{1,0:T(8,128)}, f32[768,2048]{1,0:T(8,128)S(1)}, u32[]{:S(2)}) copy-start(f32[768,2048]{1,0:T(8,128)S(1)} %get-tuple-element.10) | copy-start | bytes 18874372
  244.3 6.2 %collective-permute-start.11 = (bf16[2,192,2048]{2,1,0:T(8,128)(2,1)S(1)}, bf16[2,192,2048]{2,1,0:T(8,128)(2,1)S(1)}, u32[]{:S(2)}, u32[]{:S(2)}) collective-permute-start(bf16[2,192,2048]{2,1,0:T(8,128)(2,1)S(1)} %pad_maximum_fusion.1), channel_id=1, source_target_pairs={{0,1},{1,0},{2,3},{3,2},{4,5},{5,4},{6,7},{7,6},{8,9},{9,8},{10,11... | collective-permute-start | bytes 4718600 | tf_op jit(solution)/shard_map/ppermute | solution.py:88
  249.0 20.5 %collective-permute-start.4 = (bf16[192,2048]{1,0:T(8,128)(2,1)S(1)}, bf16[192,2048]{1,0:T(8,128)(2,1)S(1)}, u32[]{:S(2)}, u32[]{:S(2)}) collective-permute-start(bf16[192,2048]{1,0:T(8,128)(2,1)S(1)} %fusion.7), channel_id=1, source_target_pairs={{0,2},{1,3},{2,0},{3,1},{4,6},{5,7},{6,4},{7,5},{8,10},{9,11},{10,... | collective-permute-start | bytes 2359304 | tf_op jit(solution)/shard_map/ppermute | solution.py:88
  252.0 56.9 %collective-permute-start.12 = (bf16[192,2048]{1,0:T(8,128)(2,1)}, bf16[192,2048]{1,0:T(8,128)(2,1)}, u32[]{:S(2)}, u32[]{:S(2)}) collective-permute-start(bf16[192,2048]{1,0:T(8,128)(2,1)} %fusion.2), channel_id=1, source_target_pairs={{0,2},{1,3},{2,0},{3,1},{4,6},{5,7},{6,4},{7,5},{8,10},{9,11},{10,... | collective-permute-start | bytes 2359304 | tf_op jit(solution)/shard_map/ppermute | solution.py:88
  305.4 10.8 %all-to-all-start.3 = ((bf16[4,64,768]{2,1,0:T(8,128)(2,1)}), bf16[4,64,768]{2,1,0:T(8,128)(2,1)S(1)}, u32[]{:S(2)}, u32[]{:S(2)}) async-start(bf16[4,64,768]{2,1,0:T(8,128)(2,1)} %bitcast.86), calls=%async_computation.4 | async-start | bytes 786432 | tf_op jit(solution)/shard_map/all_to_all | solution.py:151
  311.7 4.7 %copy-start.7 = (f32[64,3072]{1,0:T(8,128)S(1)}, f32[64,3072]{1,0:T(8,128)}, u32[]{:S(2)}) copy-start(f32[64,3072]{1,0:T(8,128)} %param.13) | copy-start | bytes 2359300
  (2 other events, 3.1 us)
Sparse Core Ops, SparseCore 0:
  20.1 60.7 all-gather.3
  83.1 58.6 all-gather.7
  144.0 58.6 all-gather.5
  232.4 72.9 reduce-scatter.1

commit v2 on v1

--- a/solution.py
+++ b/solution.py
@@ -1,6 +1,10 @@
+import functools
+
 import jax
 import jax.numpy as jnp
 from jax import lax
+from jax.experimental import pallas as pl
+from jax.experimental.pallas import tpu as pltpu
 from jax.sharding import PartitionSpec as P
 
 QUAD = 4
@@ -88,11 +92,6 @@
     return lax.ppermute(value, "fs", [(index, index ^ bit) for index in range(total)])
 
 
-def gather_tokens(rows):
-    far = swap(rows, 2)
-    return jnp.concatenate([rows, swap(rows, 1), far, swap(far, 1)], axis=0)
-
-
 def return_tokens(partial):
     blocks = partial.astype(jnp.bfloat16).reshape(QUAD, -1, partial.shape[1])
     mine = partial.reshape(blocks.shape)
@@ -100,25 +99,179 @@
     far = swap((mine[2] + near[1]).astype(jnp.bfloat16), 2)
     return (mine[0] + near[0] + far.astype(jnp.float32)).astype(jnp.bfloat16)
 
-
-def gather_weight(weight):
-    total = lax.axis_size("fs")
-    part = lax.all_to_all(
-        weight, "fs", split_axis=1, concat_axis=0, tiled=True, axis_index_groups=quads_of(total)
-    )
-    return lax.all_gather(part, "fs", axis=0, tiled=True, axis_index_groups=lanes_of(total))
+def ring_group(place, ring):
+    half = lax.div(2 * place, ring)
+    return 2 * place * (1 - half) + (2 * (ring - 1 - place) + 1) * half
+
+
+def ring_place(group, ring):
+    odd = lax.rem(group, 2)
+    return lax.div(group, 2) * (1 - odd) + (ring - 1 - lax.div(group, 2)) * odd
+
+
+def gather_kernel(ring, weights, tokens, *refs):
+    weight_refs, token_refs = refs[:weights], refs[weights : weights + tokens]
+    outs = refs[weights + tokens : 2 * (weights + tokens)]
+    whole_refs, rows_refs = outs[:weights], outs[weights:]
+    ring_send, ring_recv, quad_send, quad_recv, token_send, token_recv, local_sem = refs[
+        2 * (weights + tokens) :
+    ]
+    me = lax.axis_index("fs")
+    group, lane = lax.div(me, QUAD), lax.rem(me, QUAD)
+    low, high = lax.rem(lane, 2), lax.div(lane, 2)
+    relative = [lane, lane + 1 - 2 * low, lane + 2 - 4 * high, QUAD - 1 - lane]
+    peers = [group * QUAD + other for other in relative]
+    place = ring_place(group, ring)
+    around = [
+        ring_group(lax.rem(place + shift, ring), ring) * QUAD + lane for shift in (1, ring - 1)
+    ]
+    depth = weight_refs[0].shape[0]
+    width = weight_refs[0].shape[1] // QUAD
+
+    barrier = pltpu.get_barrier_semaphore()
+    for other in peers[1:] + around:
+        pl.semaphore_signal(
+            barrier, inc=1, device_id={"fs": other}, device_id_type=pl.DeviceIdType.MESH
+        )
+    pl.semaphore_wait(barrier, QUAD + 1)
+
+    def remote(source, target, send, recv, other):
+        return pltpu.make_async_remote_copy(
+            src_ref=source,
+            dst_ref=target,
+            send_sem=send,
+            recv_sem=recv,
+            device_id={"fs": other},
+            device_id_type=pl.DeviceIdType.MESH,
+        )
+
+    def slab(weight, owner, member):
+        first = pl.multiple_of((owner * QUAD + member) * depth, depth)
+        return whole_refs[weight].at[pl.ds(first, depth), :]
+
+    def columns(weight, member):
+        return weight_refs[weight].at[:, pl.ds(pl.multiple_of(member * width, width), width)]
+
+    sent, kept = [], []
+    quad, hops, rows = {}, {}, {}
+    for weight in range(weights):
+        for far in (3, 2, 1):
+            copy = remote(
+                columns(weight, relative[far]),
+                slab(weight, group, lane),
+                quad_send.at[weight, far - 1],
+                quad_recv.at[weight, far - 1],
+                peers[far],
+            )
+            copy.start()
+            quad[weight, far] = copy
+            sent.append(copy)
+    for weight in range(weights):
+        copy = pltpu.make_async_copy(
+            columns(weight, lane), slab(weight, group, lane), local_sem.at[weight]
+        )
+        copy.start()
+        kept.append(copy)
+
+    def row_block(token, block):
+        count = token_refs[token].shape[0]
+        return rows_refs[token].at[pl.ds(block * count, count), :]
+
+    def send_rows(token, source, block, slot, other):
+        copy = remote(
+            source,
+            row_block(token, block),
+            token_send.at[token, slot],
+            token_recv.at[token, slot],
+            other,
+        )
+        copy.start()
+        rows[token, slot] = copy
+        sent.append(copy)
+
+    for token in range(tokens):
+        send_rows(token, token_refs[token], 2, 1, peers[2])
+    for token in range(tokens):
+        send_rows(token, token_refs[token], 1, 0, peers[1])
+        copy = pltpu.make_async_copy(
+            token_refs[token], row_block(token, 0), local_sem.at[weights + token]
+        )
+        copy.start()
+        kept.append(copy)
+
+    for step in range(ring - 1):
+        for weight in range(weights):
+            for piece in (0, 1, 3, 2):
+                if step:
+                    hops[weight, piece, step - 1].wait_recv()
+                elif piece:
+                    quad[weight, piece].wait_recv()
+                forward = piece in (0, 3)
+                back = ring - step if forward else step
+                owner = ring_group(lax.rem(place + back, ring), ring)
+                target = slab(weight, owner, relative[piece])
+                copy = remote(
+                    columns(weight, lane) if step == 0 and piece == 0 else target,
+                    target,
+                    ring_send.at[weight, piece, step],
+                    ring_recv.at[weight, piece, step],
+                    around[0 if forward else 1],
+                )
+                copy.start()
+                hops[weight, piece, step] = copy
+                sent.append(copy)
+        for token in range(tokens):
+            if step == ring - 2 - 2 * (tokens - 1 - token):
+                rows[token, 1].wait_recv()
+                send_rows(token, row_block(token, 2), 3, 2, peers[1])
+    for weight in range(weights):
+        for piece in range(QUAD):
+            hops[weight, piece, ring - 2].wait_recv()
+    for token in range(tokens):
+        rows[token, 0].wait_recv()
+        rows[token, 2].wait_recv()
+    for copy in sent:
+        copy.wait_send()
+    for copy in kept:
+        copy.wait()
+
+
+def gather(identity, weight_list, token_list):
+    ring = lax.axis_size("fs") // QUAD
+    weights, tokens = len(weight_list), len(token_list)
+    dma = pltpu.SemaphoreType.DMA
+    outs = [
+        jax.ShapeDtypeStruct((w.shape[0] * QUAD * ring, w.shape[1] // QUAD), w.dtype)
+        for w in weight_list
+    ] + [jax.ShapeDtypeStruct((t.shape[0] * QUAD, t.shape[1]), t.dtype) for t in token_list]
+    return pl.pallas_call(
+        functools.partial(gather_kernel, ring, weights, tokens),
+        out_shape=outs,
+        in_specs=[pl.BlockSpec(memory_space=pltpu.VMEM)] * (weights + tokens),
+        out_specs=[pl.BlockSpec(memory_space=pl.ANY)] * (weights + tokens),
+        scratch_shapes=[
+            dma((weights, QUAD, ring - 1)),
+            dma((weights, QUAD, ring - 1)),
+            dma((weights, QUAD - 1)),
+            dma((weights, QUAD - 1)),
+            dma((tokens, 3)),
+            dma((tokens, 3)),
+            dma((weights + tokens,)),
+        ],
+        compiler_params=pltpu.CompilerParams(collective_id=identity, has_side_effects=True),
+        cost_estimate=pl.CostEstimate(
+            flops=0, bytes_accessed=weights * 90_000_000, transcendentals=0
+        ),
+    )(*weight_list, *token_list)
 
 
 def quad_shards(
     later_input, earlier_input, cotangent, gate_weight, up_weight, down_weight, down_grad_sum
 ):
     total = lax.axis_size("fs")
-    gate_whole = gather_weight(gate_weight)
-    up_whole = gather_weight(up_weight)
-    down_whole = gather_weight(down_weight)
-    early_rows = gather_tokens(earlier_input)
-    grad_rows = gather_tokens(cotangent)
-    later_rows = gather_tokens(later_input)
+    gate_whole, up_whole, early_rows, grad_rows = gather(
+        0, (gate_weight, up_weight), (earlier_input, cotangent)
+    )
 
     gate_early = jnp.dot(early_rows, gate_whole, preferred_element_type=jnp.float32)
     up_early = jnp.dot(early_rows, up_whole, preferred_element_type=jnp.float32)
@@ -135,6 +288,10 @@
         tiled=True,
         axis_index_groups=lanes_of(total),
     )
+    held_weight, held_input, _ = lax.optimization_barrier(
+        (down_weight, later_input, partial_sum)
+    )
+    down_whole, later_rows = gather(1, (held_weight,), (held_input,))
     gate_later = jnp.dot(later_rows, gate_whole, preferred_element_type=jnp.float32)
     up_later = jnp.dot(later_rows, up_whole, preferred_element_type=jnp.float32)
     hidden_later = (jax.nn.silu(gate_later) * up_later).astype(jnp.bfloat16)

time: 324 us -> 243 us (0.75)
  waiting for transfers between devices: 198 us -> 27.2 us
  Pallas kernels: 0 us -> 135 us
  blocking collectives: 32.5 us -> 0 us
  local copies, waits for them, and re-layouts: 12.8 us -> 4.72 us
    pallas_call x0 -> x2, Pallas kernels: none -> 135 us  [gather(): pl.pallas_call(functools.partial(gather_kernel, ring, weights, tokens), o...]
    all_gather x3 -> x0, waiting for transfers between devices: 94.2 us -> none  [gather_weight(): lax.all_gather(part, 'fs', axis=0, tiled=True, axis_index_groups=lanes_of...]
    ppermute x13 -> x4, waiting for transfers between devices: 66.4 us -> 26.4 us  [swap(): lax.ppermute(value, 'fs', [(index, index ^ bit) for index in range(total)])]
    reduce_scatter x1, waiting for transfers between devices: 33.3 us -> 0.01 us  [quad_shards(): lax.psum_scatter(partial_sum, 'fs', scatter_dimension=0, tiled=True, axis...]
    all_to_all x3 -> x0, blocking collectives: 32.5 us -> none  [gather_weight(): lax.all_to_all(weight, 'fs', split_axis=1, concat_axis=0, tiled=True, axi...]
    unnamed x41 -> x20, local copies, waits for them, and re-layouts: 9.03 us -> 3.01 us
    all_to_all x1, waiting for transfers between devices: 4.55 us -> 0.82 us  [quad_shards(): lax.all_to_all(summed, 'fs', split_axis=0, concat_axis=1, tiled=True, axi...]
  transfers between devices with their start and end apart: 18 -> 6, of which waited for: 9 -> 3; matrix products, arithmetic and copies ran while one was open for 15% -> 18% of each run, Pallas kernels for 0% -> 26%
where the time goes in v2:
time: 243 us
  Pallas kernels  135 us (56%)
  matrix products  41.4 us (17%)
  waiting for transfers between devices  27.2 us (11%)
  between operations  14.3 us (6%)
  other arithmetic  14.1 us (6%)
  starting transfers between devices  5.69 us (2%)
  local copies, waits for them, and re-layouts  4.72 us (2%)
    pallas_call x2, Pallas kernels, gather(): pl.pallas_call(functools.partial(gather_kernel, ring, weights, tokens), o...  135 us
    ppermute x4, waiting for transfers between devices, swap(): lax.ppermute(value, 'fs', [(index, index ^ bit) for index in range(total)])  26.4 us
    dot_general x3, matrix products, contract_last(): lax.dot_general(leading, trailing, (((1,), (1,)), ((), ())), preferred_el...  19 us
    dot_general x1, matrix products, quad_shards(): jnp.dot(grad_rows, down_whole, preferred_element_type=jnp.float32)  5.71 us
    dot_general x1, matrix products, quad_shards(): jnp.dot(early_rows, gate_whole, preferred_element_type=jnp.float32)  5.58 us
    convert_element_type x2, other arithmetic, return_tokens(): return (mine[0] + near[0] + far.astype(jnp.float32)).astype(jnp.bfloat16)  5.44 us
  transfers between devices with their start and end apart: 6, of which 3 were waited for; matrix products, arithmetic and copies ran while one was open for 18% of the time, Pallas kernels for 26%

profile of v2, /device:TPU:0, one launch (start us, length us, event | category | flops | bytes accessed | tf_op | source)
XLA Modules:
  0.0 242.6 jit_solution(12736472913772901298)
XLA Ops:
  7.2 71.6 %shard_map.94 = (bf16[2048,768]{1,0:T(8,128)(2,1)}, bf16[2048,768]{1,0:T(8,128)(2,1)}, bf16[768,2048]{1,0:T(8,128)(2,1)}, bf16[768,2048]{1,0:T(8,128)(2,1)}) custom-call(bf16[64,3072]{1,0:T(8,128)(2,1)} %refs_0_.1, bf16[64,3072]{1,0:T(8,128)(2,1)} %refs_1_.1, bf16[192,2048]{1,0:T(8,128)(2,1)} %refs_2_.1, bf16[192,2048]{1,0:T(8,128)(2,1)} %refs_3_.1), custom_call_target="tpu_custom_call" | custom-call | bytes 180000000 | tf_op jit(solution)/shard_map/pallas_call | solution.py:247
  78.8 5.6 %fusion.22 = f32[768,768]{1,0:T(8,128)S(1)} fusion(bf16[768,2048]{1,0:T(8,128)(2,1)} %get-tuple-element.12, bf16[2048,768]{1,0:T(8,128)(2,1)} %get-tuple-element.13), kind=kOutput, calls=%fused_computation.38 | convolution fusion | flops 2415919104 | bytes 8650752 | tf_op jit(solution)/shard_map/dot_general | solution.py:276
  84.5 2.6 %fusion.23 = f32[768,768]{1,0:T(8,128)S(1)} fusion(bf16[768,2048]{1,0:T(8,128)(2,1)S(1)} %copy-done.7, bf16[2048,768]{1,0:T(8,128)(2,1)S(1)} %copy-done), kind=kOutput, calls=%fused_computation.39 | convolution fusion | flops 2415919104 | bytes 8650752 | tf_op jit(solution)/shard_map/dot_general | solution.py:277
  87.1 1.5 copy-done.8
  88.6 4.4 %convolution_convert_fusion = bf16[2048,768]{1,0:T(8,128)(2,1)} fusion(bf16[768,2048]{1,0:T(8,128)(2,1)S(1)} %copy-done.6, f32[768,768]{1,0:T(8,128)S(1)} %fusion.23, f32[768,768]{1,0:T(8,128)S(1)} %fusion.22), kind=kOutput, calls=%fused_computation.1 | convolution fusion | flops 2421030912 | bytes 11010048 | tf_op jit(solution)/shard_map/dot_general | solution.py:281
  93.0 63.5 %shard_map.95 = (bf16[2048,768]{1,0:T(8,128)(2,1)}, bf16[768,2048]{1,0:T(8,128)(2,1)}) custom-call(bf16[64,3072]{1,0:T(8,128)(2,1)} %refs_0_.2, bf16[192,2048]{1,0:T(8,128)(2,1)} %refs_1_.2), custom_call_target="tpu_custom_call" | custom-call | bytes 90000000 | tf_op jit(solution)/shard_map/pallas_call | solution.py:247
  156.5 5.7 %fusion.25 = f32[768,768]{1,0:T(8,128)S(1)} fusion(bf16[768,2048]{1,0:T(8,128)(2,1)} %get-tuple-element.11, bf16[2048,768]{1,0:T(8,128)(2,1)} %get-tuple-element.18), kind=kOutput, calls=%fused_computation.41 | convolution fusion | flops 2415919104 | bytes 8650752 | tf_op jit(solution)/shard_map/dot_general | solution.py:299
  162.3 3.3 %fusion.11 = f32[768,2048]{1,0:T(8,128)S(1)} fusion(bf16[2048,768]{1,0:T(8,128)(2,1)S(1)} %copy-done.4, f32[768,768]{1,0:T(8,128)S(1)} %copy-done.2, f32[768,768]{1,0:T(8,128)S(1)} %fusion.25, f32[768,768]{1,0:T(8,128)S(1)} %copy-done.9), kind=kOutput, calls=%fused_computation.24 | convolution fusion | flops 2421817344 | bytes 16515072 | tf_op jit(solution)/shard_map/dot_general | solution.py:14
  165.5 4.7 %fusion.21 = (bf16[768,2048]{1,0:T(8,128)(2,1)S(1)}, f32[768,2048]{1,0:T(8,128)}) fusion(f32[768,2048]{1,0:T(8,128)S(1)} %fusion.11, bf16[2048,768]{1,0:T(8,128)(2,1)S(1)} %copy-done, f32[768,768]{1,0:T(8,128)S(1)} %fusion.25, f32[768,768]{1,0:T(8,128)S(1)} %copy-done.2), kind=kOutput, calls=%fused_computation.37 | convolution fusion | flops 2422603776 | bytes 23592960 | tf_op jit(solution)/shard_map/dot_general | solution.py:14
  170.2 0.2 slice_bitcast_fusion.5
  170.4 1.3 pad_maximum_fusion.1
  171.7 1.4 copy-done.5
  173.1 4.1 %fusion.24 = f32[768,768]{1,0:T(8,128)} fusion(bf16[768,2048]{1,0:T(8,128)(2,1)S(1)} %copy-done.5, bf16[2048,768]{1,0:T(8,128)(2,1)S(1)} %copy-done.4), kind=kOutput, calls=%fused_computation.40 | convolution fusion | flops 2415919104 | bytes 8650752 | tf_op jit(solution)/shard_map/dot_general | solution.py:295
  177.2 11.1 %fusion.20 = (bf16[768,2048]{1,0:T(8,128)(2,1)}, f32[768,2048]{1,0:T(8,128)}) fusion(bf16[2048,768]{1,0:T(8,128)(2,1)} %get-tuple-element.18, f32[768,768]{1,0:T(8,128)} %fusion.24, bf16[768,2048]{1,0:T(8,128)(2,1)} %get-tuple-element.17, bf16[2048,768]{1,0:T(8,128)(2,1)S(1)} %copy-done), kind=kOutput, calls=%fused_computation.36 | convolution fusion | flops 4836950016 | bytes 21233664 | tf_op jit(solution)/shard_map/dot_general | solution.py:14
  188.2 1.5 slice_bitcast_fusion.7
  189.7 0.1 pad_maximum_fusion
  189.9 0.1 collective-permute-start
  190.0 1.8 convert_element_type.61
  191.7 1.6 fusion.2
  193.4 1.2 collective-permute-start.3
  194.6 0.4 convert_element_type.54
  195.0 2.5 %fusion.7 = bf16[192,2048]{1,0:T(8,128)(2,1)} fusion(f32[2,192,2048]{2,1,0:T(8,128)S(1)} %convert_element_type.54, f32[768,2048]{1,0:T(8,128)} %get-tuple-element.24), kind=kLoop, calls=%fused_computation.17 | loop fusion | flops 786432 | bytes 3932160 | tf_op jit(solution)/shard_map/convert_element_type | solution.py:99
  197.4 0.9 collective-permute-start.1
  198.3 15.5 %collective-permute-done.3 = bf16[192,2048]{1,0:T(8,128)(2,1)S(1)} collective-permute-done((bf16[192,2048]{1,0:T(8,128)(2,1)S(1)}, bf16[192,2048]{1,0:T(8,128)(2,1)S(1)}, u32[]{:S(2)}, u32[]{:S(2)}) %collective-permute-start.3) | collective-permute-done | bytes 786464 | tf_op jit(solution)/shard_map/ppermute | solution.py:92
  213.8 2.6 %fusion.5 = bf16[192,2048]{1,0:T(8,128)(2,1)} fusion(f32[2,192,2048]{2,1,0:T(8,128)S(1)} %convert_element_type.61, f32[768,2048]{1,0:T(8,128)} %get-tuple-element.26, bf16[192,2048]{1,0:T(8,128)(2,1)S(1)} %collective-permute-done.3), kind=kLoop, calls=%fused_computation.14 | loop fusion | flops 1572864 | bytes 4718592 | tf_op jit(solution)/shard_map/convert_element_type | solution.py:100
  216.5 3.5 %all-to-all-start = ((bf16[4,64,768]{2,1,0:T(8,128)(2,1)}), bf16[4,64,768]{2,1,0:T(8,128)(2,1)S(1)}, u32[]{:S(2)}, u32[]{:S(2)}) async-start(bf16[4,64,768]{2,1,0:T(8,128)(2,1)} %bitcast.56), calls=%async_computation.1 | async-start | bytes 786432 | tf_op jit(solution)/shard_map/all_to_all | solution.py:308
  220.0 10.9 %collective-permute-done.1 = bf16[192,2048]{1,0:T(8,128)(2,1)} collective-permute-done((bf16[192,2048]{1,0:T(8,128)(2,1)}, bf16[192,2048]{1,0:T(8,128)(2,1)}, u32[]{:S(2)}, u32[]{:S(2)}) %collective-permute-start.1) | collective-permute-done | bytes 786464 | tf_op jit(solution)/shard_map/ppermute | solution.py:92
  230.8 2.8 %fusion.10 = bf16[192,2048]{1,0:T(8,128)(2,1)} fusion(f32[2,192,2048]{2,1,0:T(8,128)S(1)} %convert_element_type.54, f32[768,2048]{1,0:T(8,128)} %get-tuple-element.24, bf16[192,2048]{1,0:T(8,128)(2,1)} %collective-permute-done.1), kind=kLoop, calls=%fused_computation.21 | loop fusion | flops 1572864 | bytes 4718592 | tf_op jit(solution)/shard_map/convert_element_type | solution.py:100
  233.6 0.8 all-to-all-done
  234.4 0.1 multiply_bitcast_fusion
  234.6 0.2 copy-done.3
  234.8 1.0 add.46
  (24 shorter events, 0.2 us)
Async XLA Ops:
  7.2 209.3 %reduce-scatter.2.cloned.1.call-start = ((), (), s32[]{:S(2)}) async-start(), calls=%async_computation.2 | async-start | bytes 3538944 | tf_op jit(solution)/shard_map/reduce_scatter | solution.py:284
  78.8 5.6 %copy-start = (bf16[2048,768]{1,0:T(8,128)(2,1)S(1)}, bf16[2048,768]{1,0:T(8,128)(2,1)}, u32[]{:S(2)}) copy-start(bf16[2048,768]{1,0:T(8,128)(2,1)} %get-tuple-element.14) | copy-start | bytes 9437188
  78.8 5.6 %copy-start.7 = (bf16[768,2048]{1,0:T(8,128)(2,1)S(1)}, bf16[768,2048]{1,0:T(8,128)(2,1)}, u32[]{:S(2)}) copy-start(bf16[768,2048]{1,0:T(8,128)(2,1)} %get-tuple-element.12) | copy-start | bytes 9437188
  84.4 2.7 %copy-start.1 = (f32[768,768]{1,0:T(8,128)}, f32[768,768]{1,0:T(8,128)S(1)}, u32[]{:S(2)}) copy-start(f32[768,768]{1,0:T(8,128)S(1)} %fusion.22) | copy-start | bytes 7077892
  84.4 4.1 %copy-start.6 = (bf16[768,2048]{1,0:T(8,128)(2,1)S(1)}, bf16[768,2048]{1,0:T(8,128)(2,1)}, u32[]{:S(2)}) copy-start(bf16[768,2048]{1,0:T(8,128)(2,1)} %get-tuple-element.11) | copy-start | bytes 9437188
  87.1 1.5 copy-start.8
  156.5 5.7 %copy-start.2 = (f32[768,768]{1,0:T(8,128)S(1)}, f32[768,768]{1,0:T(8,128)}, u32[]{:S(2)}) copy-start(f32[768,768]{1,0:T(8,128)} %copy-done.1) | copy-start | bytes 7077892
  156.5 5.7 %copy-start.4 = (bf16[2048,768]{1,0:T(8,128)(2,1)S(1)}, bf16[2048,768]{1,0:T(8,128)(2,1)}, u32[]{:S(2)}) copy-start(bf16[2048,768]{1,0:T(8,128)(2,1)} %get-tuple-element.13) | copy-start | bytes 9437188
  156.5 5.7 %copy-start.9 = (f32[768,768]{1,0:T(8,128)S(1)}, f32[768,768]{1,0:T(8,128)}, u32[]{:S(2)}) copy-start(f32[768,768]{1,0:T(8,128)} %copy-done.8) | copy-start | bytes 7077892
  170.4 2.7 %copy-start.5 = (bf16[768,2048]{1,0:T(8,128)(2,1)S(1)}, bf16[768,2048]{1,0:T(8,128)(2,1)}, u32[]{:S(2)}) copy-start(bf16[768,2048]{1,0:T(8,128)(2,1)} %get-tuple-element.17) | copy-start | bytes 9437188
  171.7 18.3 %collective-permute-start.2 = (bf16[2,192,2048]{2,1,0:T(8,128)(2,1)}, bf16[2,192,2048]{2,1,0:T(8,128)(2,1)}, u32[]{:S(2)}, u32[]{:S(2)}) collective-permute-start(bf16[2,192,2048]{2,1,0:T(8,128)(2,1)} %pad_maximum_fusion.1), channel_id=1, source_target_pairs={{0,1},{1,0},{2,3},{3,2},{4,5},{5,4},{6,7},{7,6},{8,9},{9,8},{10,11... | collective-permute-start | bytes 4718600 | tf_op jit(solution)/shard_map/ppermute | solution.py:92
  189.9 4.7 %collective-permute-start = (bf16[2,192,2048]{2,1,0:T(8,128)(2,1)S(1)}, bf16[2,192,2048]{2,1,0:T(8,128)(2,1)S(1)}, u32[]{:S(2)}, u32[]{:S(2)}) collective-permute-start(bf16[2,192,2048]{2,1,0:T(8,128)(2,1)S(1)} %pad_maximum_fusion), channel_id=1, source_target_pairs={{0,1},{1,0},{2,3},{3,2},{4,5},{5,4},{6,7},{7,6},{8,9},{9,8},{10,11... | collective-permute-start | bytes 4718600 | tf_op jit(solution)/shard_map/ppermute | solution.py:92
  193.4 20.5 %collective-permute-start.3 = (bf16[192,2048]{1,0:T(8,128)(2,1)S(1)}, bf16[192,2048]{1,0:T(8,128)(2,1)S(1)}, u32[]{:S(2)}, u32[]{:S(2)}) collective-permute-start(bf16[192,2048]{1,0:T(8,128)(2,1)S(1)} %fusion.2), channel_id=1, source_target_pairs={{0,2},{1,3},{2,0},{3,1},{4,6},{5,7},{6,4},{7,5},{8,10},{9,11},{10,... | collective-permute-start | bytes 2359304 | tf_op jit(solution)/shard_map/ppermute | solution.py:92
  197.4 33.4 %collective-permute-start.1 = (bf16[192,2048]{1,0:T(8,128)(2,1)}, bf16[192,2048]{1,0:T(8,128)(2,1)}, u32[]{:S(2)}, u32[]{:S(2)}) collective-permute-start(bf16[192,2048]{1,0:T(8,128)(2,1)} %fusion.7), channel_id=1, source_target_pairs={{0,2},{1,3},{2,0},{3,1},{4,6},{5,7},{6,4},{7,5},{8,10},{9,11},{10,... | collective-permute-start | bytes 2359304 | tf_op jit(solution)/shard_map/ppermute | solution.py:92
  216.5 18.0 %all-to-all-start = ((bf16[4,64,768]{2,1,0:T(8,128)(2,1)}), bf16[4,64,768]{2,1,0:T(8,128)(2,1)S(1)}, u32[]{:S(2)}, u32[]{:S(2)}) async-start(bf16[4,64,768]{2,1,0:T(8,128)(2,1)} %bitcast.56), calls=%async_computation.1 | async-start | bytes 786432 | tf_op jit(solution)/shard_map/all_to_all | solution.py:308
  233.6 1.1 copy-start.3
Sparse Core Ops, SparseCore 0:
  93.1 95.7 reduce-scatter.1

commit v3 on v2

--- a/solution.py
+++ b/solution.py
@@ -269,8 +269,8 @@
     later_input, earlier_input, cotangent, gate_weight, up_weight, down_weight, down_grad_sum
 ):
     total = lax.axis_size("fs")
-    gate_whole, up_whole, early_rows, grad_rows = gather(
-        0, (gate_weight, up_weight), (earlier_input, cotangent)
+    gate_whole, up_whole, down_whole, early_rows, grad_rows, later_rows = gather(
+        0, (gate_weight, up_weight, down_weight), (earlier_input, cotangent, later_input)
     )
 
     gate_early = jnp.dot(early_rows, gate_whole, preferred_element_type=jnp.float32)
@@ -288,10 +288,9 @@
         tiled=True,
         axis_index_groups=lanes_of(total),
     )
-    held_weight, held_input, _ = lax.optimization_barrier(
-        (down_weight, later_input, partial_sum)
-    )
-    down_whole, later_rows = gather(1, (held_weight,), (held_input,))
+    down_whole, later_rows, _ = lax.optimization_barrier(
+        (down_whole, later_rows, partial_sum)
+    )
     gate_later = jnp.dot(later_rows, gate_whole, preferred_element_type=jnp.float32)
     up_later = jnp.dot(later_rows, up_whole, preferred_element_type=jnp.float32)
     hidden_later = (jax.nn.silu(gate_later) * up_later).astype(jnp.bfloat16)

time: 243 us -> 217 us (0.89)
  Pallas kernels: 135 us -> 102 us
  waiting for transfers between devices: 27.2 us -> 34.4 us
    pallas_call x2 -> x1, Pallas kernels: 135 us -> 102 us  [gather(): pl.pallas_call(functools.partial(gather_kernel, ring, weights, tokens), o...]
    reduce_scatter x1, waiting for transfers between devices: 0.01 us -> 14.3 us  [quad_shards(): lax.psum_scatter(partial_sum, 'fs', scatter_dimension=0, tiled=True, axis...]
    ppermute x4, waiting for transfers between devices: 26.4 us -> 15.6 us  [swap(): lax.ppermute(value, 'fs', [(index, index ^ bit) for index in range(total)])]
    all_to_all x1, waiting for transfers between devices: 0.82 us -> 4.55 us  [quad_shards(): lax.all_to_all(summed, 'fs', split_axis=0, concat_axis=1, tiled=True, axi...]
  transfers between devices with their start and end apart: 6 -> 6, of which waited for: 3 -> 3; matrix products, arithmetic and copies ran while one was open for 18% -> 20% of each run, Pallas kernels for 26% -> 0%
where the time goes in v3:
time: 217 us; the launch traced here: 216 us
  Pallas kernels  102 us (47%)
  matrix products  41.3 us (19%)
  waiting for transfers between devices  34.4 us (16%)
  between operations  14.3 us (7%)
  other arithmetic  14.2 us (7%)
  starting transfers between devices  5.66 us (3%)
  local copies, waits for them, and re-layouts  4.39 us (2%)
    pallas_call x1, Pallas kernels, gather(): pl.pallas_call(functools.partial(gather_kernel, ring, weights, tokens), o...  102 us
    dot_general x3, matrix products, contract_last(): lax.dot_general(leading, trailing, (((1,), (1,)), ((), ())), preferred_el...  19 us
    ppermute x4, waiting for transfers between devices, swap(): lax.ppermute(value, 'fs', [(index, index ^ bit) for index in range(total)])  15.6 us
    reduce_scatter x1, waiting for transfers between devices, quad_shards(): lax.psum_scatter(partial_sum, 'fs', scatter_dimension=0, tiled=True, axis...  14.3 us
    dot_general x1, matrix products, quad_shards(): jnp.dot(grad_rows, down_whole, preferred_element_type=jnp.float32)  5.58 us
    dot_general x1, matrix products, quad_shards(): jnp.dot(early_rows, gate_whole, preferred_element_type=jnp.float32)  5.58 us
    convert_element_type x2, other arithmetic, return_tokens(): return (mine[0] + near[0] + far.astype(jnp.float32)).astype(jnp.bfloat16)  5.47 us
    all_to_all x1, waiting for transfers between devices, quad_shards(): lax.all_to_all(summed, 'fs', split_axis=0, concat_axis=1, tiled=True, axi...  4.55 us
  transfers between devices with their start and end apart: 6, of which 3 were waited for; matrix products, arithmetic and copies ran while one was open for 20% of the time, Pallas kernels for 0%

profile of v3, /device:TPU:0, one launch (start us, length us, event | category | flops | bytes accessed | tf_op | source)
XLA Modules:
  0.0 216.4 jit_solution(6152215082142050151)
XLA Ops:
  7.2 0.0 reduce-scatter.2.cloned.1.call-start
  7.2 102.1 %shard_map.94 = (bf16[2048,768]{1,0:T(8,128)(2,1)}, bf16[2048,768]{1,0:T(8,128)(2,1)}, bf16[2048,768]{1,0:T(8,128)(2,1)}, bf16[768,2048]{1,0:T(8,128)(2,1)}, bf1...) custom-call(bf16[64,3072]{1,0:T(8,128)(2,1)} %refs_0_.1, bf16[64,3072]{1,0:T(8,128)(2,1)} %refs_1_.1, ...), custom_call_target="tpu_custom_call" | custom-call | bytes 270000000 | tf_op jit(solution)/shard_map/pallas_call | solution.py:247
  109.4 5.6 %fusion.22 = f32[768,768]{1,0:T(8,128)S(1)} fusion(bf16[768,2048]{1,0:T(8,128)(2,1)} %get-tuple-element.14, bf16[2048,768]{1,0:T(8,128)(2,1)} %get-tuple-element.15), kind=kOutput, calls=%fused_computation.38 | convolution fusion | flops 2415919104 | bytes 8650752 | tf_op jit(solution)/shard_map/dot_general | solution.py:276
  115.0 2.6 %fusion.23 = f32[768,768]{1,0:T(8,128)S(1)} fusion(bf16[768,2048]{1,0:T(8,128)(2,1)S(1)} %copy-done.7, bf16[2048,768]{1,0:T(8,128)(2,1)S(1)} %copy-done), kind=kOutput, calls=%fused_computation.39 | convolution fusion | flops 2415919104 | bytes 8650752 | tf_op jit(solution)/shard_map/dot_general | solution.py:277
  117.6 1.5 copy-done.8
  119.1 4.4 %convolution_convert_fusion = bf16[2048,768]{1,0:T(8,128)(2,1)} fusion(bf16[768,2048]{1,0:T(8,128)(2,1)S(1)} %copy-done.6, f32[768,768]{1,0:T(8,128)S(1)} %fusion.23, f32[768,768]{1,0:T(8,128)S(1)} %fusion.22), kind=kOutput, calls=%fused_computation.1 | convolution fusion | flops 2421030912 | bytes 11010048 | tf_op jit(solution)/shard_map/dot_general | solution.py:281
  123.6 5.6 %fusion.25 = f32[768,768]{1,0:T(8,128)S(1)} fusion(bf16[768,2048]{1,0:T(8,128)(2,1)} %get-tuple-element.13, bf16[2048,768]{1,0:T(8,128)(2,1)} %get-tuple-element.18), kind=kOutput, calls=%fused_computation.41 | convolution fusion | flops 2415919104 | bytes 8650752 | tf_op jit(solution)/shard_map/dot_general | solution.py:298
  129.2 3.3 %fusion.11 = f32[768,2048]{1,0:T(8,128)S(1)} fusion(bf16[2048,768]{1,0:T(8,128)(2,1)S(1)} %copy-done.5, f32[768,768]{1,0:T(8,128)S(1)} %copy-done.2, f32[768,768]{1,0:T(8,128)S(1)} %fusion.25, f32[768,768]{1,0:T(8,128)S(1)} %copy-done.9), kind=kOutput, calls=%fused_computation.24 | convolution fusion | flops 2421817344 | bytes 16515072 | tf_op jit(solution)/shard_map/dot_general | solution.py:14
  132.5 4.5 %fusion.21 = (bf16[768,2048]{1,0:T(8,128)(2,1)S(1)}, f32[768,2048]{1,0:T(8,128)}) fusion(f32[768,2048]{1,0:T(8,128)S(1)} %fusion.11, bf16[2048,768]{1,0:T(8,128)(2,1)S(1)} %copy-done, f32[768,768]{1,0:T(8,128)S(1)} %fusion.25, f32[768,768]{1,0:T(8,128)S(1)} %copy-done.2), kind=kOutput, calls=%fused_computation.37 | convolution fusion | flops 2422603776 | bytes 23592960 | tf_op jit(solution)/shard_map/dot_general | solution.py:14
  137.0 0.2 slice_bitcast_fusion.5
  137.2 1.3 pad_maximum_fusion.1
  138.5 1.2 copy-done.4
  139.6 4.1 %fusion.24 = f32[768,768]{1,0:T(8,128)} fusion(bf16[768,2048]{1,0:T(8,128)(2,1)S(1)} %copy-done.4, bf16[2048,768]{1,0:T(8,128)(2,1)S(1)} %copy-done.5), kind=kOutput, calls=%fused_computation.40 | convolution fusion | flops 2415919104 | bytes 8650752 | tf_op jit(solution)/shard_map/dot_general | solution.py:294
  143.8 11.2 %fusion.20 = (bf16[768,2048]{1,0:T(8,128)(2,1)}, f32[768,2048]{1,0:T(8,128)}) fusion(bf16[2048,768]{1,0:T(8,128)(2,1)} %get-tuple-element.18, f32[768,768]{1,0:T(8,128)} %fusion.24, bf16[768,2048]{1,0:T(8,128)(2,1)} %get-tuple-element.17, bf16[2048,768]{1,0:T(8,128)(2,1)S(1)} %copy-done), kind=kOutput, calls=%fused_computation.36 | convolution fusion | flops 4836950016 | bytes 21233664 | tf_op jit(solution)/shard_map/dot_general | solution.py:14
  154.9 1.5 slice_bitcast_fusion.7
  156.4 0.1 pad_maximum_fusion
  156.6 0.1 collective-permute-start
  156.7 1.8 convert_element_type.61
  158.5 1.7 fusion.2
  160.1 0.8 collective-permute-start.3
  160.9 0.4 convert_element_type.54
  161.3 2.5 %fusion.7 = bf16[192,2048]{1,0:T(8,128)(2,1)} fusion(f32[2,192,2048]{2,1,0:T(8,128)S(1)} %convert_element_type.54, f32[768,2048]{1,0:T(8,128)} %get-tuple-element.24), kind=kLoop, calls=%fused_computation.17 | loop fusion | flops 786432 | bytes 3932160 | tf_op jit(solution)/shard_map/convert_element_type | solution.py:99
  163.8 1.3 collective-permute-start.1
  165.1 15.5 %collective-permute-done.3 = bf16[192,2048]{1,0:T(8,128)(2,1)S(1)} collective-permute-done((bf16[192,2048]{1,0:T(8,128)(2,1)S(1)}, bf16[192,2048]{1,0:T(8,128)(2,1)S(1)}, u32[]{:S(2)}, u32[]{:S(2)}) %collective-permute-start.3) | collective-permute-done | bytes 786464 | tf_op jit(solution)/shard_map/ppermute | solution.py:92
  180.6 2.7 %fusion.5 = bf16[192,2048]{1,0:T(8,128)(2,1)} fusion(f32[2,192,2048]{2,1,0:T(8,128)S(1)} %convert_element_type.61, f32[768,2048]{1,0:T(8,128)} %get-tuple-element.26, bf16[192,2048]{1,0:T(8,128)(2,1)S(1)} %collective-permute-done.3), kind=kLoop, calls=%fused_computation.14 | loop fusion | flops 1572864 | bytes 4718592 | tf_op jit(solution)/shard_map/convert_element_type | solution.py:100
  183.3 14.3 %reduce-scatter.2.cloned.1.call-done = bf16[256,768]{1,0:T(8,128)(2,1)} async-done(((bf16[2048,768]{1,0:T(8,128)(2,1)}), bf16[256,768]{1,0:T(8,128)(2,1)}) %reduce-scatter.2.cloned.1.call-update) | async-done | bytes 393232 | tf_op jit(solution)/shard_map/reduce_scatter | solution.py:284
  197.6 3.5 %all-to-all-start = ((bf16[4,64,768]{2,1,0:T(8,128)(2,1)}), bf16[4,64,768]{2,1,0:T(8,128)(2,1)S(1)}, u32[]{:S(2)}, u32[]{:S(2)}) async-start(bf16[4,64,768]{2,1,0:T(8,128)(2,1)} %bitcast.56), calls=%async_computation.1 | async-start | bytes 786432 | tf_op jit(solution)/shard_map/all_to_all | solution.py:307
  201.1 2.8 %fusion.10 = bf16[192,2048]{1,0:T(8,128)(2,1)} fusion(f32[2,192,2048]{2,1,0:T(8,128)S(1)} %convert_element_type.54, f32[768,2048]{1,0:T(8,128)} %get-tuple-element.24, bf16[192,2048]{1,0:T(8,128)(2,1)} %collective-permute-done.1), kind=kLoop, calls=%fused_computation.21 | loop fusion | flops 1572864 | bytes 4718592 | tf_op jit(solution)/shard_map/convert_element_type | solution.py:100
  203.9 4.6 %all-to-all-done = bf16[4,64,768]{2,1,0:T(8,128)(2,1)S(1)} async-done(((bf16[4,64,768]{2,1,0:T(8,128)(2,1)}), bf16[4,64,768]{2,1,0:T(8,128)(2,1)S(1)}, u32[]{:S(2)}, u32[]{:S(2)}) %all-to-all-start) | async-done | bytes 393248 | tf_op jit(solution)/shard_map/all_to_all | solution.py:307
  208.4 0.1 multiply_bitcast_fusion
  208.5 0.1 copy.11
  208.6 1.0 add.46
  (23 shorter events, 0.1 us)
Async XLA Ops:
  7.2 190.4 %reduce-scatter.2.cloned.1.call-start = ((), (), s32[]{:S(2)}) async-start(), calls=%async_computation.2 | async-start | bytes 3538944 | tf_op jit(solution)/shard_map/reduce_scatter | solution.py:284
  109.3 5.6 %copy-start = (bf16[2048,768]{1,0:T(8,128)(2,1)S(1)}, bf16[2048,768]{1,0:T(8,128)(2,1)}, u32[]{:S(2)}) copy-start(bf16[2048,768]{1,0:T(8,128)(2,1)} %get-tuple-element.16) | copy-start | bytes 9437188
  109.4 5.6 %copy-start.7 = (bf16[768,2048]{1,0:T(8,128)(2,1)S(1)}, bf16[768,2048]{1,0:T(8,128)(2,1)}, u32[]{:S(2)}) copy-start(bf16[768,2048]{1,0:T(8,128)(2,1)} %get-tuple-element.14) | copy-start | bytes 9437188
  114.9 2.7 %copy-start.1 = (f32[768,768]{1,0:T(8,128)}, f32[768,768]{1,0:T(8,128)S(1)}, u32[]{:S(2)}) copy-start(f32[768,768]{1,0:T(8,128)S(1)} %fusion.22) | copy-start | bytes 7077892
  115.0 4.1 %copy-start.6 = (bf16[768,2048]{1,0:T(8,128)(2,1)S(1)}, bf16[768,2048]{1,0:T(8,128)(2,1)}, u32[]{:S(2)}) copy-start(bf16[768,2048]{1,0:T(8,128)(2,1)} %get-tuple-element.13) | copy-start | bytes 9437188
  117.6 1.5 copy-start.8
  123.6 5.6 %copy-start.2 = (f32[768,768]{1,0:T(8,128)S(1)}, f32[768,768]{1,0:T(8,128)}, u32[]{:S(2)}) copy-start(f32[768,768]{1,0:T(8,128)} %copy-done.1) | copy-start | bytes 7077892
  123.6 5.6 %copy-start.5 = (bf16[2048,768]{1,0:T(8,128)(2,1)S(1)}, bf16[2048,768]{1,0:T(8,128)(2,1)}, u32[]{:S(2)}) copy-start(bf16[2048,768]{1,0:T(8,128)(2,1)} %get-tuple-element.15) | copy-start | bytes 9437188
  123.6 5.6 %copy-start.9 = (f32[768,768]{1,0:T(8,128)S(1)}, f32[768,768]{1,0:T(8,128)}, u32[]{:S(2)}) copy-start(f32[768,768]{1,0:T(8,128)} %copy-done.8) | copy-start | bytes 7077892
  137.2 2.5 %copy-start.4 = (bf16[768,2048]{1,0:T(8,128)(2,1)S(1)}, bf16[768,2048]{1,0:T(8,128)(2,1)}, u32[]{:S(2)}) copy-start(bf16[768,2048]{1,0:T(8,128)(2,1)} %get-tuple-element.17) | copy-start | bytes 9437188
  138.5 18.2 %collective-permute-start.2 = (bf16[2,192,2048]{2,1,0:T(8,128)(2,1)}, bf16[2,192,2048]{2,1,0:T(8,128)(2,1)}, u32[]{:S(2)}, u32[]{:S(2)}) collective-permute-start(bf16[2,192,2048]{2,1,0:T(8,128)(2,1)} %pad_maximum_fusion.1), channel_id=1, source_target_pairs={{0,1},{1,0},{2,3},{3,2},{4,5},{5,4},{6,7},{7,6},{8,9},{9,8},{10,11... | collective-permute-start | bytes 4718600 | tf_op jit(solution)/shard_map/ppermute | solution.py:92
  156.6 4.3 %collective-permute-start = (bf16[2,192,2048]{2,1,0:T(8,128)(2,1)S(1)}, bf16[2,192,2048]{2,1,0:T(8,128)(2,1)S(1)}, u32[]{:S(2)}, u32[]{:S(2)}) collective-permute-start(bf16[2,192,2048]{2,1,0:T(8,128)(2,1)S(1)} %pad_maximum_fusion), channel_id=1, source_target_pairs={{0,1},{1,0},{2,3},{3,2},{4,5},{5,4},{6,7},{7,6},{8,9},{9,8},{10,11... | collective-permute-start | bytes 4718600 | tf_op jit(solution)/shard_map/ppermute | solution.py:92
  160.1 20.5 %collective-permute-start.3 = (bf16[192,2048]{1,0:T(8,128)(2,1)S(1)}, bf16[192,2048]{1,0:T(8,128)(2,1)S(1)}, u32[]{:S(2)}, u32[]{:S(2)}) collective-permute-start(bf16[192,2048]{1,0:T(8,128)(2,1)S(1)} %fusion.2), channel_id=1, source_target_pairs={{0,2},{1,3},{2,0},{3,1},{4,6},{5,7},{6,4},{7,5},{8,10},{9,11},{10,... | collective-permute-start | bytes 2359304 | tf_op jit(solution)/shard_map/ppermute | solution.py:92
  163.8 37.3 %collective-permute-start.1 = (bf16[192,2048]{1,0:T(8,128)(2,1)}, bf16[192,2048]{1,0:T(8,128)(2,1)}, u32[]{:S(2)}, u32[]{:S(2)}) collective-permute-start(bf16[192,2048]{1,0:T(8,128)(2,1)} %fusion.7), channel_id=1, source_target_pairs={{0,2},{1,3},{2,0},{3,1},{4,6},{5,7},{6,4},{7,5},{8,10},{9,11},{10,... | collective-permute-start | bytes 2359304 | tf_op jit(solution)/shard_map/ppermute | solution.py:92
  197.6 10.8 %all-to-all-start = ((bf16[4,64,768]{2,1,0:T(8,128)(2,1)}), bf16[4,64,768]{2,1,0:T(8,128)(2,1)S(1)}, u32[]{:S(2)}, u32[]{:S(2)}) async-start(bf16[4,64,768]{2,1,0:T(8,128)(2,1)} %bitcast.56), calls=%async_computation.1 | async-start | bytes 786432 | tf_op jit(solution)/shard_map/all_to_all | solution.py:307
  203.9 4.7 %copy-start.3 = (f32[64,3072]{1,0:T(8,128)S(1)}, f32[64,3072]{1,0:T(8,128)}, u32[]{:S(2)}) copy-start(f32[64,3072]{1,0:T(8,128)} %param.13) | copy-start | bytes 2359300
Sparse Core Ops, SparseCore 0:
  123.7 73.8 reduce-scatter.1
